TPU v7x, 256 devices: a whole 4x4x8 slice. The times are simulated.
256 devices in a mesh: sp: 16 (over y, x), dp: 16 (over z, core).
Axes of the slice: x: 4, y: 4, z: 8, core: 2. Of those that a mesh axis runs over, the one named last changes fastest.
Arguments:
- value_half: bfloat16 [16, 4096, 2048], P('dp', 'sp'), may hold values from -6 to 6
- gate_half: bfloat16 [16, 4096, 2048], P('dp', 'sp'), may hold values from -6 to 6
- upstream: bfloat16 [16, 4096, 2048], P('dp', 'sp'), may hold values from -6 to 6
- conv_taps: float32 [31, 2048], P(None, 'sp'), may hold values from -1 to 1
- norm_gain: float32 [2048], replicated, may hold values from 0.1 to 1.9
- out_weight: bfloat16 [2048, 2048], P('dp'), may hold values from -0.125 to 0.125
Outputs:
- grad_value: bfloat16 [16, 4096, 2048], P('dp', 'sp')
- grad_gate: bfloat16 [16, 4096, 2048], P('dp', 'sp')
- grad_taps: float32 [31, 2048], P(None, 'sp')
- grad_gain: float32 [2048], replicated
- grad_weight: float32 [2048, 2048], P('dp')
All inputs are finite; a program needn't handle non-finite values.
Results may differ from a plain program's by a relative error of at most 0.0062.
Values may be sent and summed in bfloat16 or wider, within the bound.
A program may use at most 128 MiB of HBM per device.

v0:
```python
import functools
import jax
import jax.numpy as jnp
from jax import lax
from jax.sharding import Mesh
from jax.sharding import PartitionSpec as P

DP = ("dp_0", "dp_1")
SP = ("sp_0", "sp_1")
SP_DP = ("sp_0", "sp_1", "dp_0", "dp_1")
NORM_EPS = 1e-05


def from_everyone(shard, axis):
    count = lax.axis_size(axis)
    return lax.all_to_all(
        jnp.broadcast_to(shard[None], (count, *shard.shape)), axis, 0, 0, tiled=True
    )


def of_everyone(shard, axis):
    return from_everyone(shard, axis).sum(axis=0)


def one_axis_at_a_time(shard, axes):
    return functools.reduce(lax.psum, axes, shard)


def body(value_half, gate_half, upstream, conv_taps, norm_gain, out_weight):
    tap_count = conv_taps.shape[0]
    sig_gate = jax.nn.sigmoid(gate_half.astype(jnp.float32))
    value_wide = value_half.astype(jnp.float32)
    glu = (value_wide * sig_gate).astype(jnp.bfloat16)
    glu_heads = lax.all_to_all(glu, SP, split_axis=2, concat_axis=1, tiled=True).astype(jnp.float32)
    length = glu_heads.shape[1]
    padded = jnp.pad(glu_heads, ((0, 0), (tap_count - 1, 0), (0, 0)))
    conv_out = jnp.zeros_like(glu_heads)
    for offset in range(tap_count):
        conv_out = conv_out + conv_taps[offset] * padded[:, offset : offset + length]
    conv_tokens = lax.all_to_all(
        conv_out.astype(jnp.bfloat16), SP, split_axis=1, concat_axis=2, tiled=True
    ).astype(jnp.float32)
    row_mean = jnp.mean(conv_tokens, axis=-1, keepdims=True)
    centered = conv_tokens - row_mean
    inv_scale = lax.rsqrt(jnp.mean(centered * centered, axis=-1, keepdims=True) + NORM_EPS)
    normed = centered * inv_scale
    scaled = normed * norm_gain
    sig_scaled = jax.nn.sigmoid(scaled)
    activated = (scaled * sig_scaled).astype(jnp.bfloat16)[0]
    upstream_rows = upstream[0]
    columns = upstream_rows
    grad_act = jnp.dot(
        columns,
        lax.all_gather(out_weight, DP, axis=0, tiled=True),
        preferred_element_type=jnp.float32,
    )
    grad_scaled = grad_act[None] * sig_scaled * (1.0 + scaled * (1.0 - sig_scaled))
    gain_part = jnp.sum(grad_scaled * normed, axis=(0, 1))
    grad_normed = grad_scaled * norm_gain
    grad_conv_out = inv_scale * (
        grad_normed
        - jnp.mean(grad_normed, axis=-1, keepdims=True)
        - normed * jnp.mean(grad_normed * normed, axis=-1, keepdims=True)
    )
    grad_heads = lax.all_to_all(
        grad_conv_out.astype(jnp.bfloat16), SP, split_axis=2, concat_axis=1, tiled=True
    ).astype(jnp.float32)
    grad_padded = jnp.pad(grad_heads, ((0, 0), (0, tap_count - 1), (0, 0)))
    grad_glu = jnp.zeros_like(grad_heads)
    tap_terms = []
    for offset in range(tap_count):
        first = tap_count - 1 - offset
        grad_glu = grad_glu + conv_taps[offset] * grad_padded[:, first : first + length]
        tap_terms.append(jnp.sum(grad_heads * padded[:, offset : offset + length], axis=(0, 1)))
    grad_taps = of_everyone(jnp.stack(tap_terms), DP)
    grad_tokens = lax.all_to_all(
        grad_glu.astype(jnp.bfloat16), SP, split_axis=1, concat_axis=2, tiled=True
    ).astype(jnp.float32)
    grad_value = (grad_tokens * sig_gate).astype(jnp.bfloat16)
    grad_gate = (grad_tokens * value_wide * sig_gate * (1.0 - sig_gate)).astype(jnp.bfloat16)
    grad_gain = one_axis_at_a_time(gain_part, SP_DP)
    columns = upstream_rows
    owned = lax.psum_scatter(
        lax.dot_general(
            columns, activated, (((0,), (0,)), ((), ())), preferred_element_type=jnp.float32
        ),
        DP,
        scatter_dimension=0,
        tiled=True,
    )
    grad_weight = lax.psum(owned, SP)
    return (grad_value, grad_gate, grad_taps, grad_gain, grad_weight)


def solution(mesh):
    torus = Mesh(mesh.devices.reshape(4, 4, 8, 2), ("sp_0", "sp_1", "dp_0", "dp_1"))
    placed = (P(DP, SP, None), P(DP, SP, None), P(DP, SP, None), P(None, SP), P(), P(DP, None))
    return jax.shard_map(
        body,
        mesh=torus,
        in_specs=placed,
        out_specs=(P(DP, SP, None), P(DP, SP, None), P(None, SP), P(), P(DP, None)),
        check_vma=False,
    )
```

profile of v0, /device:TPU:32, one launch (start us, length us, event | category | flops | bytes accessed | tf_op | source)
XLA Modules:
  0.0 445.5 jit_solution(18143520017637400832)
XLA Ops:
  7.2 0.7 all-gather.2.cloned.1.call-update
  7.9 1.5 copy.75
  9.4 1.9 copy.76
  11.3 0.6 fusion.1
  11.9 12.9 %copy.120 = bf16[1,256,2048]{1,0,2:T(2,128)(2,1)} copy(bf16[1,256,2048]{1,2,0:T(8,128)(2,1)S(1)} %fusion.1) | data formatting | bytes 2097152 | tf_op jit(solution)/shard_map/convert_element_type | solution.py:33
  24.8 0.5 broadcast.202
  25.3 11.6 %reduce.17 = bf16[2048,256]{1,0:T(8,128)(2,1)S(1)} reduce(bf16[2048,1,256]{2,1,0:T(2,128)(2,1)} %bitcast.226, bf16[]{:T(256)} %broadcast.202), dimensions={1}, to_apply=%bitcast.207.reduce_sub_computation | reduce | bytes 2097154
  37.0 1.1 reshape.390
  38.1 7.1 %all-to-all-start = ((bf16[16,2,16384]{2,1,0:T(2,128)(2,1)}), bf16[16,2,16384]{2,1,0:T(2,128)(2,1)}, u32[]{:S(2)}, u32[]{:S(2)}) async-start(bf16[16,2,16384]{2,1,0:T(2,128)(2,1)} %reshape.390), calls=%async_computation | async-start | bytes 2097152 | tf_op jit(solution)/shard_map/all_to_all | solution.py:34
  45.2 0.2 reduce-scatter.2.cloned.1.call-start
  45.5 17.5 %all-to-all-done = bf16[16,2,16384]{2,1,0:T(2,128)(2,1)} async-done(((bf16[16,2,16384]{2,1,0:T(2,128)(2,1)}), bf16[16,2,16384]{2,1,0:T(2,128)(2,1)}, u32[]{:S(2)}, u32[]{:S(2)}) %all-to-all-start) | async-done | bytes 1048608 | tf_op jit(solution)/shard_map/all_to_all | solution.py:34
  62.9 4.3 reshape.391
  67.2 1.6 copy_convert_fusion.2
  68.8 0.4 copy-done.4
  69.2 1.9 copy.79
  71.1 8.6 %add_convert_fusion.1 = bf16[1,4096,128]{2,1,0:T(8,128)(2,1)S(1)} fusion(f32[128]{0:T(128)S(1)} %get-tuple-element.104, f32[128]{0:T(128)S(1)} %get-tuple-element.105, f32[128]{0:T(128)S(1)} %get-tuple-element.76, f32[128]{0:T(128)S(1)} %get-tuple-element.77, f32[128]{0:T(128)S(1)} %get-tuple-element.78, f32[128]{0:T(128)S(1)} %get-tuple-element.79, ...), kind=kLoop, calls=%fused_computation.83 | loop fusion | flops 32505856 | bytes 5258752 | tf_op jit(solution)/shard_map/convert_element_type | solution.py:41
  79.7 17.1 %copy.119 = bf16[1,4096,128]{2,0,1:T(2,128)(2,1)} copy(bf16[1,4096,128]{2,1,0:T(8,128)(2,1)S(1)} %add_convert_fusion.1) | data formatting | bytes 2097152 | tf_op jit(solution)/shard_map/convert_element_type | solution.py:41
  96.7 24.4 %reduce.18 = bf16[4096,128]{1,0:T(8,128)(2,1)} reduce(bf16[4096,1,128]{2,1,0:T(2,128)(2,1)} %bitcast.228, bf16[]{:T(256)} %broadcast.202), dimensions={1}, to_apply=%bitcast.206.reduce_sub_computation | reduce | bytes 2097154
  121.1 2.1 reshape.392
  123.2 20.4 %all_to_all.20 = bf16[16,2,16384]{2,1,0:T(2,128)(2,1)} all-to-all(bf16[16,2,16384]{2,1,0:T(2,128)(2,1)} %reshape.392), channel_id=1, replica_groups=mesh['sp_0'=4,'sp_1'=4,'dp_0'=8,'dp_1'=2] {'sp_0','sp_1'}, dimensions={0} | all-to-all | bytes 2097152 | tf_op jit(solution)/shard_map/all_to_all | solution.py:40
  143.6 5.8 %reshape.393 = bf16[4096,1,128]{2,1,0:T(2,128)(2,1)} reshape(bf16[16,2,16384]{2,1,0:T(2,128)(2,1)} %all_to_all.20) | data formatting | bytes 2097152
  149.4 2.2 fusion.33
  151.6 3.0 copy_convert_fusion.1
  154.6 2.9 copy.82
  157.6 2.0 fusion.11
  159.8 1.8 fusion.29
  161.6 2.3 copy.91
  163.9 9.3 %convolution_bitcast_fusion = f32[2048,2048]{0,1:T(8,128)} fusion(bf16[256,2048]{0,1:T(8,128)(2,1)} %bitcast.233, bf16[1,256,2048]{2,1,0:T(8,128)(2,1)S(1)} %copy-done), kind=kOutput, calls=%fused_computation | convolution fusion | flops 2147483648 | bytes 18874368 | tf_op jit(solution)/shard_map/dot_general | solution.py:84
  173.2 4.2 copy.83
  177.4 7.7 %multiply_reduce_fusion = (f32[2048]{0:T(1024)S(1)}, f32[256]{0:T(256)S(1)}, f32[256]{0:T(256)S(1)}, f32[256,2048]{1,0:T(8,128)S(1)}) fusion(f32[256]{0:T(256)S(1)} %add_rsqrt_fusion, f32[256]{0:T(256)S(1)} %broadcast_multiply_fusion.2, f32[32,8,16,128]{3,2,1,0:T(8,128)} %bitcast.224, f32[2048]{0:T(1024)S(1)} %copy-done.10, ...), kind=kOutput, calls=%fused_computation.22 | convolution fusion | flops 2156393984 | bytes 13651968 | tf_op jit(solution)/shard_map/dot_general | solution.py:52
  185.1 1.1 fusion.30
  186.1 3.8 copy.84
  189.9 12.1 %reduce.19 = bf16[2048,256]{1,0:T(8,128)(2,1)S(1)} reduce(bf16[2048,1,256]{2,1,0:T(2,128)(2,1)} %bitcast.229, bf16[]{:T(256)} %broadcast.202), dimensions={1}, to_apply=%bitcast.194.reduce_sub_computation | reduce | bytes 2097154
  202.0 1.1 reshape.394
  203.1 18.8 %all_to_all.42 = bf16[16,2,16384]{2,1,0:T(2,128)(2,1)S(1)} all-to-all(bf16[16,2,16384]{2,1,0:T(2,128)(2,1)} %reshape.394), channel_id=1, replica_groups=mesh['sp_0'=4,'sp_1'=4,'dp_0'=8,'dp_1'=2] {'sp_0','sp_1'}, dimensions={0} | all-to-all | bytes 2097152 | tf_op jit(solution)/shard_map/all_to_all | solution.py:65
  221.9 3.5 reshape.395
  225.3 3.1 copy_convert_fusion
  228.4 2.9 copy.86
  231.4 2.8 multiply_reduce_fusion.1
  234.4 0.8 multiply_reduce_fusion.5
  235.2 2.5 multiply_reduce_fusion.2
  237.7 2.5 multiply_reduce_fusion.4
  240.2 2.5 multiply_reduce_fusion.3
  242.9 0.7 broadcast_in_dim.2
  243.6 8.5 %all-to-all-start.4 = ((f32[16,31,128]{2,1,0:T(8,128)}), f32[16,31,128]{2,1,0:T(8,128)S(1)}, u32[]{:S(2)}, u32[]{:S(2)}) async-start(f32[16,31,128]{2,1,0:T(8,128)} %broadcast_in_dim.2), calls=%async_computation.4 | async-start | bytes 524288 | tf_op jit(solution)/shard_map/all_to_all | solution.py:16
  252.1 37.3 %add_convert_fusion = bf16[1,4096,128]{2,1,0:T(8,128)(2,1)S(1)} fusion(f32[1,4096,128]{2,1,0:T(8,128)} %bitcast.213, f32[128]{0:T(128)S(1)} %get-tuple-element.104, f32[128]{0:T(128)S(1)} %get-tuple-element.105, f32[128]{0:T(128)S(1)} %get-tuple-element.76, f32[128]{0:T(128)S(1)} %get-tuple-element.77, f32[128]{0:T(128)S(1)} %get-tuple-element.78, ...), kind=kLoop, calls=%fused_computation.54 | loop fusion | flops 32505856 | bytes 3161600 | tf_op jit(solution)/shard_map/convert_element_type | solution.py:77
  289.4 16.7 %copy.118 = bf16[1,4096,128]{2,0,1:T(2,128)(2,1)S(1)} copy(bf16[1,4096,128]{2,1,0:T(8,128)(2,1)S(1)} %add_convert_fusion) | data formatting | bytes 2097152 | tf_op jit(solution)/shard_map/convert_element_type | solution.py:77
  306.1 22.4 %reduce.20 = bf16[4096,128]{1,0:T(8,128)(2,1)S(1)} reduce(bf16[4096,1,128]{2,1,0:T(2,128)(2,1)S(1)} %bitcast.227, bf16[]{:T(256)} %broadcast.202), dimensions={1}, to_apply=%bitcast.205.reduce_sub_computation | reduce | bytes 2097154
  328.5 1.1 reshape.396
  329.6 3.7 all-to-all-start.3
  333.4 0.7 all-reduce.4.cloned.1.call-update
  334.0 13.9 %psum.35 = f32[2048]{0:T(1024)S(1)} all-reduce(f32[2048]{0:T(1024)S(1)} %get-tuple-element.40), channel_id=1, replica_groups=mesh['sp_0'=4,'sp_1'=4,'dp_0'=8,'dp_1'=2] {'sp_0'}, use_global_device_ids=true, to_apply=%region_39.40 | all-reduce | flops 2048 | bytes 16384 | tf_op jit(solution)/shard_map/psum | solution.py:26
  348.0 13.8 %psum.36 = f32[2048]{0:T(1024)S(1)} all-reduce(f32[2048]{0:T(1024)S(1)} %psum.35), channel_id=1, replica_groups=mesh['sp_0'=4,'sp_1'=4,'dp_0'=8,'dp_1'=2] {'sp_1'}, use_global_device_ids=true, to_apply=%region_40.41 | all-reduce | flops 2048 | bytes 16384 | tf_op jit(solution)/shard_map/psum | solution.py:26
  361.8 15.9 %psum.37 = f32[2048]{0:T(1024)S(1)} all-reduce(f32[2048]{0:T(1024)S(1)} %psum.36), channel_id=1, replica_groups=mesh['sp_0'=4,'sp_1'=4,'dp_0'=8,'dp_1'=2] {'dp_0'}, use_global_device_ids=true, to_apply=%region_41.42 | all-reduce | flops 2048 | bytes 16384 | tf_op jit(solution)/shard_map/psum | solution.py:26
  377.7 3.1 psum.38
  380.8 0.6 reduce_sum.386
  381.4 1.0 reshape.397
  382.6 1.5 convert_bitcast_fusion
  384.1 3.1 copy.89
  387.2 3.4 fusion.4
  390.6 2.3 copy.93
  392.9 1.4 copy.92
  394.3 42.0 %all-reduce.4.cloned.1.call-done = f32[128,2048]{0,1:T(8,128)} async-done(((f32[128,2048]{0,1:T(8,128)}), f32[128,2048]{0,1:T(8,128)}) %all-reduce.4.cloned.1.call-update) | async-done | bytes 1048592 | tf_op jit(solution)/shard_map/psum | solution.py:91
  436.3 2.5 copy.94
  (40 shorter events, 0.8 us)
Async XLA Ops:
  7.2 156.7 %copy-start = (bf16[1,256,2048]{2,1,0:T(8,128)(2,1)S(1)}, bf16[1,256,2048]{2,1,0:T(8,128)(2,1)}, u32[]{:S(2)}) copy-start(bf16[1,256,2048]{2,1,0:T(8,128)(2,1)} %param.8) | copy-start | bytes 3145732
  7.2 170.2 %all-gather.2.cloned.1.call-start = ((), (), s32[]{:S(2)}) async-start(), calls=%async_computation.6 | async-start | bytes 8912896 | tf_op jit(solution)/shard_map/all_gather | solution.py:54
  9.4 2.5 copy-start.5
  11.3 13.5 %copy-start.7 = (bf16[1,256,2048]{1,2,0:T(8,128)(2,1)}, bf16[1,256,2048]{1,2,0:T(8,128)(2,1)S(1)}, u32[]{:S(2)}) copy-start(bf16[1,256,2048]{1,2,0:T(8,128)(2,1)S(1)} %copy.76) | copy-start | bytes 3145732
  37.0 8.4 %copy-start.11 = (f32[31,128]{1,0:T(8,128)S(1)}, f32[31,128]{1,0:T(8,128)}, u32[]{:S(2)}) copy-start(f32[31,128]{1,0:T(8,128)} %param.9) | copy-start | bytes 47620
  38.1 24.8 %all-to-all-start = ((bf16[16,2,16384]{2,1,0:T(2,128)(2,1)}), bf16[16,2,16384]{2,1,0:T(2,128)(2,1)}, u32[]{:S(2)}, u32[]{:S(2)}) async-start(bf16[16,2,16384]{2,1,0:T(2,128)(2,1)} %reshape.390), calls=%async_computation | async-start | bytes 2097152 | tf_op jit(solution)/shard_map/all_to_all | solution.py:34
  45.2 288.2 %reduce-scatter.2.cloned.1.call-start = ((), (), s32[]{:S(2)}) async-start(), calls=%async_computation.7 | async-start | bytes 17825792 | tf_op jit(solution)/shard_map/reduce_scatter | solution.py:83
  67.2 2.0 copy-start.4
  157.6 2.1 copy-start.10
  157.6 2.2 copy-start.3
  177.4 7.7 %copy-start.9 = (f32[1,256,16,128]{3,2,1,0:T(8,128)S(1)}, f32[1,256,16,128]{3,2,1,0:T(8,128)}, u32[]{:S(2)}) copy-start(f32[1,256,16,128]{3,2,1,0:T(8,128)} %copy.83) | copy-start | bytes 6291460
  231.4 3.0 copy-start.2
  243.6 86.0 %all-to-all-start.4 = ((f32[16,31,128]{2,1,0:T(8,128)}), f32[16,31,128]{2,1,0:T(8,128)S(1)}, u32[]{:S(2)}, u32[]{:S(2)}) async-start(f32[16,31,128]{2,1,0:T(8,128)} %broadcast_in_dim.2), calls=%async_computation.4 | async-start | bytes 524288 | tf_op jit(solution)/shard_map/all_to_all | solution.py:16
  329.6 51.8 %all-to-all-start.3 = ((bf16[16,2,16384]{2,1,0:T(2,128)(2,1)}), bf16[16,2,16384]{2,1,0:T(2,128)(2,1)S(1)}, u32[]{:S(2)}, u32[]{:S(2)}) async-start(bf16[16,2,16384]{2,1,0:T(2,128)(2,1)} %reshape.396), calls=%async_computation.3 | async-start | bytes 2097152 | tf_op jit(solution)/shard_map/all_to_all | solution.py:76
  333.3 103.0 %all-reduce.4.cloned.1.call-start = ((), (), s32[]{:S(2)}) async-start(), calls=%async_computation.8 | async-start | bytes 2097152 | tf_op jit(solution)/shard_map/psum | solution.py:91
  384.1 3.1 copy-start.6
  384.1 3.1 copy-start.8
  392.9 45.9 %copy-start.1 = (bf16[1,256,2048]{2,1,0:T(8,128)(2,1)S(1)}, bf16[1,256,2048]{2,1,0:T(8,128)(2,1)}, u32[]{:S(2)}) copy-start(bf16[1,256,2048]{2,1,0:T(8,128)(2,1)} %param.8) | copy-start | bytes 3145732
Sparse Core Ops, SparseCore 0:
  9.8 56.6 all-gather.1
  173.3 101.6 reduce-scatter.1
  337.3 98.8 all-reduce.3
where the time goes:
time: 452 us; the launch traced here: 446 us
  other arithmetic  148 us (33%)
  local copies, waits for them, and re-layouts  99.6 us (22%)
  blocking collectives  85.9 us (19%)
  waiting for transfers between devices  60.8 us (13%)
  starting transfers between devices  19.5 us (4%)
  matrix products  17 us (4%)
  between operations  14.2 us (3%)
    unnamed x4, other arithmetic  70.5 us
    psum x4, blocking collectives, one_axis_at_a_time(): return functools.reduce(lax.psum, axes, shard)  46.7 us
    psum x1, waiting for transfers between devices, body(): grad_weight = lax.psum(owned, SP)  42 us
    convert_element_type x1, other arithmetic, body(): grad_glu.astype(jnp.bfloat16)  37.3 us
    unnamed x38, local copies, waits for them, and re-layouts  30.8 us
    all_to_all x1, blocking collectives, body(): lax.all_to_all(conv_out.astype(jnp.bfloat16), SP, split_axis=1, concat_ax...  20.4 us
    all_to_all x1, blocking collectives, body(): lax.all_to_all(grad_conv_out.astype(jnp.bfloat16), SP, split_axis=2, conc...  18.8 us
    all_to_all x1, waiting for transfers between devices, body(): lax.all_to_all(glu, SP, split_axis=2, concat_axis=1, tiled=True)  17.5 us
  transfers between devices with their start and end apart: 6, of which 2 were waited for; matrix products, arithmetic and copies ran while one was open for 59% of the time, Pallas kernels for 0%

commit v1 on v0

--- a/solution.py
+++ b/solution.py
@@ -88,7 +88,7 @@
         scatter_dimension=0,
         tiled=True,
     )
-    grad_weight = lax.psum(owned, SP)
+    grad_weight = jnp.sum(lax.all_gather(owned, SP), axis=0)
     return (grad_value, grad_gate, grad_taps, grad_gain, grad_weight)
 
 

time: 452 us -> 589 us (1.30)
  waiting for transfers between devices: 60.8 us -> 167 us
  other arithmetic: 148 us -> 159 us
  blocking collectives: 85.9 us -> 94.9 us
  local copies, waits for them, and re-layouts: 99.6 us -> 108 us
    reduce_scatter x1, waiting for transfers between devices: 0.02 us -> 95.5 us  [body(): lax.psum_scatter(lax.dot_general(columns, activated, (((0,), (0,)), ((),...]
    all_gather x1, waiting for transfers between devices: 0.01 us -> 53.7 us  [body(): lax.all_gather(out_weight, DP, axis=0, tiled=True)]
    psum x1 -> x0, waiting for transfers between devices: 42 us -> none  [body(): grad_weight = lax.psum(owned, SP)]
    reduce_sum x0 -> x1, other arithmetic: none -> 11.9 us  [body(): grad_weight = jnp.sum(lax.all_gather(owned, SP), axis=0)]
    all_to_all x1, blocking collectives: 18.8 us -> 27.3 us  [body(): lax.all_to_all(grad_conv_out.astype(jnp.bfloat16), SP, split_axis=2, conc...]
    unnamed x38 -> x41, local copies, waits for them, and re-layouts: 30.8 us -> 39.1 us
  transfers between devices with their start and end apart: 6 -> 6, of which waited for: 2 -> 3; matrix products, arithmetic and copies ran while one was open for 59% -> 24% of each run, Pallas kernels for 0% -> 0%
where the time goes in v1:
time: 589 us; the launch traced here: 580 us
  waiting for transfers between devices  167 us (28%)
  other arithmetic  159 us (27%)
  local copies, waits for them, and re-layouts  108 us (18%)
  blocking collectives  94.9 us (16%)
  starting transfers between devices  19.8 us (3%)
  matrix products  17 us (3%)
  between operations  14.3 us (2%)
    reduce_scatter x1, waiting for transfers between devices, body(): lax.psum_scatter(lax.dot_general(columns, activated, (((0,), (0,)), ((),...  95.5 us
    unnamed x4, other arithmetic  70.1 us
    all_gather x1, waiting for transfers between devices, body(): lax.all_gather(out_weight, DP, axis=0, tiled=True)  53.7 us
    psum x4, blocking collectives, one_axis_at_a_time(): return functools.reduce(lax.psum, axes, shard)  47.5 us
    unnamed x41, local copies, waits for them, and re-layouts  39.1 us
    convert_element_type x1, other arithmetic, body(): grad_glu.astype(jnp.bfloat16)  37.3 us
    all_to_all x1, blocking collectives, body(): lax.all_to_all(grad_conv_out.astype(jnp.bfloat16), SP, split_axis=2, conc...  27.3 us
    all_to_all x1, blocking collectives, body(): lax.all_to_all(conv_out.astype(jnp.bfloat16), SP, split_axis=1, concat_ax...  20.2 us
  transfers between devices with their start and end apart: 6, of which 3 were waited for; matrix products, arithmetic and copies ran while one was open for 24% of the time, Pallas kernels for 0%

profile of v1, /device:TPU:32, one launch (start us, length us, event | category | flops | bytes accessed | tf_op | source)
XLA Modules:
  0.0 579.8 jit_solution(15061841898495327684)
XLA Ops:
  7.2 1.6 copy.72
  8.8 1.9 copy.73
  10.6 0.6 fusion.1
  11.2 12.9 %copy.118 = bf16[1,256,2048]{1,0,2:T(2,128)(2,1)} copy(bf16[1,256,2048]{1,2,0:T(8,128)(2,1)S(1)} %fusion.1) | data formatting | bytes 2097152 | tf_op jit(solution)/shard_map/convert_element_type | solution.py:33
  24.2 0.5 broadcast.202
  24.7 11.6 %reduce.17 = bf16[2048,256]{1,0:T(8,128)(2,1)S(1)} reduce(bf16[2048,1,256]{2,1,0:T(2,128)(2,1)} %bitcast.232, bf16[]{:T(256)} %broadcast.202), dimensions={1}, to_apply=%bitcast.212.reduce_sub_computation | reduce | bytes 2097154
  36.3 1.1 reshape.391
  37.4 7.1 %all-to-all-start = ((bf16[16,2,16384]{2,1,0:T(2,128)(2,1)}), bf16[16,2,16384]{2,1,0:T(2,128)(2,1)}, u32[]{:S(2)}, u32[]{:S(2)}) async-start(bf16[16,2,16384]{2,1,0:T(2,128)(2,1)} %reshape.391), calls=%async_computation | async-start | bytes 2097152 | tf_op jit(solution)/shard_map/all_to_all | solution.py:34
  44.8 17.5 %all-to-all-done = bf16[16,2,16384]{2,1,0:T(2,128)(2,1)} async-done(((bf16[16,2,16384]{2,1,0:T(2,128)(2,1)}), bf16[16,2,16384]{2,1,0:T(2,128)(2,1)}, u32[]{:S(2)}, u32[]{:S(2)}) %all-to-all-start) | async-done | bytes 1048608 | tf_op jit(solution)/shard_map/all_to_all | solution.py:34
  62.3 4.3 reshape.392
  66.6 1.6 copy_convert_fusion.2
  68.5 1.9 copy.76
  70.4 8.6 %add_convert_fusion.1 = bf16[1,4096,128]{2,1,0:T(8,128)(2,1)S(1)} fusion(f32[128]{0:T(128)S(1)} %get-tuple-element.89, f32[128]{0:T(128)S(1)} %get-tuple-element.90, f32[128]{0:T(128)S(1)} %get-tuple-element.61, f32[128]{0:T(128)S(1)} %get-tuple-element.62, f32[128]{0:T(128)S(1)} %get-tuple-element.63, f32[128]{0:T(128)S(1)} %get-tuple-element.64, ...), kind=kLoop, calls=%fused_computation.84 | loop fusion | flops 32505856 | bytes 5258752 | tf_op jit(solution)/shard_map/convert_element_type | solution.py:41
  79.0 17.1 %copy.117 = bf16[1,4096,128]{2,0,1:T(2,128)(2,1)} copy(bf16[1,4096,128]{2,1,0:T(8,128)(2,1)S(1)} %add_convert_fusion.1) | data formatting | bytes 2097152 | tf_op jit(solution)/shard_map/convert_element_type | solution.py:41
  96.1 24.4 %reduce.18 = bf16[4096,128]{1,0:T(8,128)(2,1)} reduce(bf16[4096,1,128]{2,1,0:T(2,128)(2,1)} %bitcast.234, bf16[]{:T(256)} %broadcast.202), dimensions={1}, to_apply=%bitcast.211.reduce_sub_computation | reduce | bytes 2097154
  120.5 2.1 reshape.393
  122.6 20.2 %all_to_all.20 = bf16[16,2,16384]{2,1,0:T(2,128)(2,1)} all-to-all(bf16[16,2,16384]{2,1,0:T(2,128)(2,1)} %reshape.393), channel_id=1, replica_groups=mesh['sp_0'=4,'sp_1'=4,'dp_0'=8,'dp_1'=2] {'sp_0','sp_1'}, dimensions={0} | all-to-all | bytes 2097152 | tf_op jit(solution)/shard_map/all_to_all | solution.py:40
  142.7 5.8 reshape.394
  148.5 2.4 fusion.33
  150.9 1.4 copy_convert_fusion.1
  152.4 2.9 copy.79
  155.3 2.0 fusion.11
  157.6 1.8 fusion.29
  159.4 2.3 copy.88
  161.6 9.3 %convolution_bitcast_fusion = f32[2048,2048]{0,1:T(8,128)} fusion(bf16[256,2048]{0,1:T(8,128)(2,1)} %bitcast.239, bf16[1,256,2048]{2,1,0:T(8,128)(2,1)S(1)} %copy-done), kind=kOutput, calls=%fused_computation.1 | convolution fusion | flops 2147483648 | bytes 18874368 | tf_op jit(solution)/shard_map/dot_general | solution.py:84
  171.0 0.7 all-gather.4.cloned.1.call-update
  171.7 95.5 %reduce-scatter.2.cloned.1.call-done = f32[128,2048]{0,1:T(8,128)} async-done(((f32[2048,2048]{0,1:T(8,128)}), f32[128,2048]{0,1:T(8,128)}) %reduce-scatter.2.cloned.1.call-update) | async-done | bytes 1048592 | tf_op jit(solution)/shard_map/reduce_scatter | solution.py:83
  267.3 4.2 copy.80
  271.5 53.7 %all-gather.4.cloned.1.call-done = bf16[2048,2048]{1,0:T(8,128)(2,1)} async-done(((bf16[128,2048]{1,0:T(8,128)(2,1)}), bf16[2048,2048]{1,0:T(8,128)(2,1)}) %all-gather.4.cloned.1.call-update) | async-done | bytes 8388624 | tf_op jit(solution)/shard_map/all_gather | solution.py:54
  325.1 7.7 %multiply_reduce_fusion = (f32[2048]{0:T(1024)S(1)}, f32[256]{0:T(256)S(1)}, f32[256]{0:T(256)S(1)}, f32[256,2048]{1,0:T(8,128)S(1)}) fusion(f32[256]{0:T(256)S(1)} %add_rsqrt_fusion, f32[256]{0:T(256)S(1)} %broadcast_multiply_fusion.2, f32[32,8,16,128]{3,2,1,0:T(8,128)} %bitcast.230, f32[2048]{0:T(1024)S(1)} %copy-done.11, ...), kind=kOutput, calls=%fused_computation.23 | convolution fusion | flops 2156393984 | bytes 13651968 | tf_op jit(solution)/shard_map/dot_general | solution.py:52
  332.8 1.1 fusion.30
  333.9 3.8 copy.81
  337.7 11.6 %reduce.19 = bf16[2048,256]{1,0:T(8,128)(2,1)S(1)} reduce(bf16[2048,1,256]{2,1,0:T(2,128)(2,1)} %bitcast.235, bf16[]{:T(256)} %broadcast.202), dimensions={1}, to_apply=%bitcast.199.reduce_sub_computation | reduce | bytes 2097154
  349.3 1.1 reshape.395
  350.4 27.3 %all_to_all.42 = bf16[16,2,16384]{2,1,0:T(2,128)(2,1)S(1)} all-to-all(bf16[16,2,16384]{2,1,0:T(2,128)(2,1)} %reshape.395), channel_id=1, replica_groups=mesh['sp_0'=4,'sp_1'=4,'dp_0'=8,'dp_1'=2] {'sp_0','sp_1'}, dimensions={0} | all-to-all | bytes 2097152 | tf_op jit(solution)/shard_map/all_to_all | solution.py:65
  377.7 3.5 reshape.396
  381.2 3.1 copy_convert_fusion
  384.2 2.9 copy.83
  387.1 2.9 multiply_reduce_fusion.1
  390.2 0.8 multiply_reduce_fusion.5
  391.0 2.5 multiply_reduce_fusion.2
  393.6 2.5 multiply_reduce_fusion.4
  396.1 2.5 multiply_reduce_fusion.3
  398.7 0.7 broadcast_in_dim.2
  399.4 7.7 %all-to-all-start.4 = ((f32[16,31,128]{2,1,0:T(8,128)}), f32[16,31,128]{2,1,0:T(8,128)S(1)}, u32[]{:S(2)}, u32[]{:S(2)}) async-start(f32[16,31,128]{2,1,0:T(8,128)} %broadcast_in_dim.2), calls=%async_computation.4 | async-start | bytes 524288 | tf_op jit(solution)/shard_map/all_to_all | solution.py:16
  407.1 37.3 %add_convert_fusion = bf16[1,4096,128]{2,1,0:T(8,128)(2,1)S(1)} fusion(f32[1,4096,128]{2,1,0:T(8,128)} %bitcast.218, f32[128]{0:T(128)S(1)} %get-tuple-element.89, f32[128]{0:T(128)S(1)} %get-tuple-element.90, f32[128]{0:T(128)S(1)} %get-tuple-element.61, f32[128]{0:T(128)S(1)} %get-tuple-element.62, f32[128]{0:T(128)S(1)} %get-tuple-element.63, ...), kind=kLoop, calls=%fused_computation.55 | loop fusion | flops 32505856 | bytes 3161600 | tf_op jit(solution)/shard_map/convert_element_type | solution.py:77
  444.4 16.7 %copy.116 = bf16[1,4096,128]{2,0,1:T(2,128)(2,1)S(1)} copy(bf16[1,4096,128]{2,1,0:T(8,128)(2,1)S(1)} %add_convert_fusion) | data formatting | bytes 2097152 | tf_op jit(solution)/shard_map/convert_element_type | solution.py:77
  461.2 22.4 %reduce.20 = bf16[4096,128]{1,0:T(8,128)(2,1)S(1)} reduce(bf16[4096,1,128]{2,1,0:T(2,128)(2,1)S(1)} %bitcast.233, bf16[]{:T(256)} %broadcast.202), dimensions={1}, to_apply=%bitcast.210.reduce_sub_computation | reduce | bytes 2097154
  483.6 1.1 reshape.397
  484.7 4.7 all-to-all-start.3
  489.4 14.3 %psum.28 = f32[2048]{0:T(1024)S(1)} all-reduce(f32[2048]{0:T(1024)S(1)} %get-tuple-element.25), channel_id=1, replica_groups=mesh['sp_0'=4,'sp_1'=4,'dp_0'=8,'dp_1'=2] {'sp_0'}, use_global_device_ids=true, to_apply=%region_39.40 | all-reduce | flops 2048 | bytes 16384 | tf_op jit(solution)/shard_map/psum | solution.py:26
  503.7 14.0 %psum.29 = f32[2048]{0:T(1024)S(1)} all-reduce(f32[2048]{0:T(1024)S(1)} %psum.28), channel_id=1, replica_groups=mesh['sp_0'=4,'sp_1'=4,'dp_0'=8,'dp_1'=2] {'sp_1'}, use_global_device_ids=true, to_apply=%region_40.41 | all-reduce | flops 2048 | bytes 16384 | tf_op jit(solution)/shard_map/psum | solution.py:26
  517.7 15.9 %psum.30 = f32[2048]{0:T(1024)S(1)} all-reduce(f32[2048]{0:T(1024)S(1)} %psum.29), channel_id=1, replica_groups=mesh['sp_0'=4,'sp_1'=4,'dp_0'=8,'dp_1'=2] {'dp_0'}, use_global_device_ids=true, to_apply=%region_41.42 | all-reduce | flops 2048 | bytes 16384 | tf_op jit(solution)/shard_map/psum | solution.py:26
  533.6 3.3 psum.31
  536.9 0.6 reduce_sum.395
  537.5 1.0 reshape.398
  538.7 1.5 convert_bitcast_fusion
  540.2 3.1 copy.86
  543.3 3.4 fusion.4
  546.7 2.3 copy.90
  548.9 1.4 copy.89
  550.4 9.4 %copy.94 = f32[256,8,16,128]{3,2,1,0:T(8,128)S(1)} copy(f32[256,8,16,128]{3,1,2,0:T(8,128)} %bitcast.228) | data formatting | bytes 33554432
  559.8 11.9 %bitcast_reduce_fusion = f32[128,2048]{0,1:T(8,128)S(1)} fusion(f32[256,8,16,128]{3,2,1,0:T(8,128)S(1)} %copy.94), kind=kLoop, calls=%fused_computation | loop fusion | flops 3932160 | bytes 17825792 | tf_op jit(solution)/shard_map/reduce_sum | solution.py:91
  571.7 1.3 copy.91
  (44 shorter events, 1.4 us)
Async XLA Ops:
  7.2 154.5 %copy-start = (bf16[1,256,2048]{2,1,0:T(8,128)(2,1)S(1)}, bf16[1,256,2048]{2,1,0:T(8,128)(2,1)}, u32[]{:S(2)}) copy-start(bf16[1,256,2048]{2,1,0:T(8,128)(2,1)} %param.8) | copy-start | bytes 3145732
  8.8 2.5 copy-start.6
  10.6 13.5 %copy-start.8 = (bf16[1,256,2048]{1,2,0:T(8,128)(2,1)}, bf16[1,256,2048]{1,2,0:T(8,128)(2,1)S(1)}, u32[]{:S(2)}) copy-start(bf16[1,256,2048]{1,2,0:T(8,128)(2,1)S(1)} %copy.73) | copy-start | bytes 3145732
  36.3 8.4 %copy-start.12 = (f32[31,128]{1,0:T(8,128)S(1)}, f32[31,128]{1,0:T(8,128)}, u32[]{:S(2)}) copy-start(f32[31,128]{1,0:T(8,128)} %param.9) | copy-start | bytes 47620
  37.4 24.8 %all-to-all-start = ((bf16[16,2,16384]{2,1,0:T(2,128)(2,1)}), bf16[16,2,16384]{2,1,0:T(2,128)(2,1)}, u32[]{:S(2)}, u32[]{:S(2)}) async-start(bf16[16,2,16384]{2,1,0:T(2,128)(2,1)} %reshape.391), calls=%async_computation | async-start | bytes 2097152 | tf_op jit(solution)/shard_map/all_to_all | solution.py:34
  44.5 222.7 %reduce-scatter.2.cloned.1.call-start = ((), (), s32[]{:S(2)}) async-start(), calls=%async_computation.7 | async-start | bytes 17825792 | tf_op jit(solution)/shard_map/reduce_scatter | solution.py:83
  66.6 2.0 copy-start.4
  148.5 2.4 copy-start.5
  152.4 5.0 copy-start.11
  155.3 2.2 copy-start.3
  170.9 154.2 %all-gather.4.cloned.1.call-start = ((), (), s32[]{:S(2)}) async-start(), calls=%async_computation.6 | async-start | bytes 8912896 | tf_op jit(solution)/shard_map/all_gather | solution.py:54
  171.7 378.7 %all-gather.6.cloned.1.call-start = ((), (), s32[]{:S(2)}) async-start(), calls=%async_computation.8 | async-start | bytes 17825792 | tf_op jit(solution)/shard_map/all_gather | solution.py:91
  325.1 7.7 %copy-start.10 = (f32[1,256,16,128]{3,2,1,0:T(8,128)S(1)}, f32[1,256,16,128]{3,2,1,0:T(8,128)}, u32[]{:S(2)}) copy-start(f32[1,256,16,128]{3,2,1,0:T(8,128)} %copy.80) | copy-start | bytes 6291460
  387.1 3.1 copy-start.2
  399.4 85.3 %all-to-all-start.4 = ((f32[16,31,128]{2,1,0:T(8,128)}), f32[16,31,128]{2,1,0:T(8,128)S(1)}, u32[]{:S(2)}, u32[]{:S(2)}) async-start(f32[16,31,128]{2,1,0:T(8,128)} %broadcast_in_dim.2), calls=%async_computation.4 | async-start | bytes 524288 | tf_op jit(solution)/shard_map/all_to_all | solution.py:16
  484.7 52.8 %all-to-all-start.3 = ((bf16[16,2,16384]{2,1,0:T(2,128)(2,1)}), bf16[16,2,16384]{2,1,0:T(2,128)(2,1)S(1)}, u32[]{:S(2)}, u32[]{:S(2)}) async-start(bf16[16,2,16384]{2,1,0:T(2,128)(2,1)} %reshape.397), calls=%async_computation.3 | async-start | bytes 2097152 | tf_op jit(solution)/shard_map/all_to_all | solution.py:76
  540.2 3.1 copy-start.7
  540.2 3.1 copy-start.9
  559.8 13.2 %copy-start.1 = (bf16[1,256,2048]{2,1,0:T(8,128)(2,1)S(1)}, bf16[1,256,2048]{2,1,0:T(8,128)(2,1)}, u32[]{:S(2)}) copy-start(bf16[1,256,2048]{2,1,0:T(8,128)(2,1)} %param.8) | copy-start | bytes 3145732
Sparse Core Ops, SparseCore 0:
  171.1 96.1 reduce-scatter.1
  269.1 55.9 all-gather.3
  327.5 136.0 all-gather.5
